TPU v7x, 32 devices: a whole 2x2x4 slice. The times are simulated.
32 devices in a mesh: sp: 8 (over z, y), tp: 4 (over x, core).
Axes of the slice: x: 2, y: 2, z: 4, core: 2. Of those that a mesh axis runs over, the one named last changes fastest.
Arguments:
- tokens: bfloat16 [2048, 4096], P('sp'), may hold values from -6 to 6
- norm_gain: float32 [4096], replicated, may hold values from 0.1 to 1.9
- w_query: bfloat16 [4096, 512], P('sp', 'tp'), may hold values from -0.09375 to 0.09375
- w_key: bfloat16 [4096, 512], P('sp', 'tp'), may hold values from -0.09375 to 0.09375
- w_value: bfloat16 [4096, 1024], P('sp', 'tp'), may hold values from -0.09375 to 0.09375
- w_gates: bfloat16 [4096, 2, 2, 4], P(None, None, None, 'tp'), may hold values from -0.09375 to 0.09375
- input_bias: float32 [2, 4], P(None, 'tp'), may hold values from -2 to 90
- forget_bias: float32 [2, 4], P(None, 'tp'), as said below
- decay_shift: float32 [2, 2048, 4], P(None, 'sp', 'tp'), may hold values from -2.5 to 0
- head_gain: float32 [1024], P('tp'), may hold values from 0.1 to 1.9
- w_conv_b: bfloat16 [4096, 1024], P('sp', 'tp'), may hold values from -0.09375 to 0.09375
- w_conv_c: bfloat16 [4096, 1024], P('sp', 'tp'), may hold values from -0.09375 to 0.09375
- w_conv_in: bfloat16 [4096, 1024], P('sp', 'tp'), may hold values from -0.09375 to 0.09375
- conv_taps: bfloat16 [3, 1024], P(None, 'tp'), may hold values from -3.5 to 3.5
- w_out: bfloat16 [2048, 4096], P('sp', 'tp'), may hold values from -0.125 to 0.125
Outputs:
- mixed_out: bfloat16 [2048, 4096], P('sp', 'tp')
Inputs may be any that keep to these rules, and one draw needn't show every extreme that they name: `forget_bias`: at most the natural logarithm of 2048 plus 2.
All inputs are finite; a program needn't handle non-finite values.
Results may differ from a plain program's by a relative error of at most 0.02.
Values may be sent and summed in bfloat16 or wider, within the bound.
A program may use at most 128 MiB of HBM per device.

v0:
```python
import jax
import jax.numpy as jnp
from jax import lax
from jax.sharding import PartitionSpec as P

DQK = 128
DV = 256
BLOCK = 128


EPS = 1e-06
HIGH = lax.Precision.HIGHEST
LOWEST = -1e30


def carried_in(value, axis, join, neutral, backward):
    count, mine = (lax.axis_size(axis), lax.axis_index(axis))
    pieces = jax.tree.map(lambda part: lax.all_gather(part, axis), value)
    if backward:
        pieces = jax.tree.map(lambda part: part[::-1], pieces)
        mine = count - 1 - mine
    subtotal = jax.tree.map(
        lambda part, zero: jnp.full_like(part, 0) + jnp.asarray(zero, part.dtype), value, neutral
    )

    def lap(position, subtotal):
        longer = join(subtotal, jax.tree.map(lambda part: part[position], pieces))
        return jax.tree.map(lambda new, old: jnp.where(position < mine, new, old), longer, subtotal)

    return lax.fori_loop(0, count - 1, lap, subtotal)


def padded_2(value, sides, width):
    for axis, dim in sides:
        size, length = (lax.axis_size(axis), value.shape[dim])
        up = [(i, (i + 1) % size) for i in range(size - 1)]
        down = [(j, i) for i, j in up]
        last = lax.slice_in_dim(value, length - width, length, axis=dim)
        initial = lax.slice_in_dim(value, 0, width, axis=dim)
        before = lax.ppermute(last, axis, up)
        after = lax.ppermute(initial, axis, down)
        value = jnp.concatenate([before, value, after], axis=dim)
    return value


def row_norm(tokens, norm_gain):
    values = tokens.astype(jnp.float32)
    inverse_rms = lax.rsqrt(jnp.mean(values * values, axis=-1, keepdims=True) + EPS)
    return (values * inverse_rms * norm_gain).astype(jnp.bfloat16)


def to_heads(source, head_count):
    length = source.shape[0]
    return source.astype(jnp.float32).reshape(length, head_count, -1).transpose(1, 0, 2)


def combine(earlier, later):
    total_a, memory_a, normer_a, stable_a = earlier
    total_b, memory_b, normer_b, stable_b = later
    stable = jnp.maximum(stable_a + total_b, stable_b)
    weight_a = jnp.exp(stable_a + total_b - stable)
    weight_b = jnp.exp(stable_b - stable)
    memory = weight_a[..., None, None] * memory_a + weight_b[..., None, None] * memory_b
    normer = weight_a[..., None] * normer_a + weight_b[..., None] * normer_b
    return (total_a + total_b, memory, normer, stable)


def local_pass(queries, keys_all, values_all, in_gate, log_forget, backward):
    head_count, length = in_gate.shape
    block_count = length // BLOCK

    def blocked(source):
        return source.reshape((head_count, block_count, BLOCK) + source.shape[2:])

    query_block = blocked(queries)
    key_blk = blocked(keys_all)
    value_blk = blocked(values_all)
    gate_blk = blocked(in_gate)
    cumulative = jnp.cumsum(blocked(log_forget), axis=-1)
    block_total = cumulative[..., -1]
    log_update = block_total[..., None] - cumulative + gate_blk
    block_stable = jnp.max(log_update, axis=-1)
    update = jnp.exp(log_update - block_stable[..., None])
    block_memory = jnp.einsum(
        "hcsv,hcsd->hcvd", value_blk * update[..., None], key_blk, precision=HIGH
    )
    block_normer = jnp.einsum("hcs,hcsd->hcd", update, key_blk, precision=HIGH)
    identity = (
        jnp.zeros((head_count,), jnp.float32),
        jnp.zeros((head_count, DV, DQK), jnp.float32),
        jnp.zeros((head_count, DQK), jnp.float32),
        jnp.full((head_count,), LOWEST, jnp.float32),
    )
    running = identity
    prefixes = []
    for index in range(block_count):
        prefixes.append(running)
        running = combine(
            running,
            (
                block_total[:, index],
                block_memory[:, index],
                block_normer[:, index],
                block_stable[:, index],
            ),
        )
    if backward:
        incoming = carried_in(running, "sp", combine, identity, True)
    else:
        incoming = carried_in(running, "sp", combine, identity, False)
    stacked = tuple((jnp.stack(members, axis=1) for members in zip(*prefixes)))
    expanded = tuple((member[:, None] for member in incoming))
    ignored, start_memory, start_normer, start_stable = combine(expanded, stacked)
    lower_mask = jnp.tril(jnp.ones((BLOCK, BLOCK), dtype=bool))
    log_weight = jnp.where(
        lower_mask,
        cumulative[..., :, None] - cumulative[..., None, :] + gate_blk[..., None, :],
        -jnp.inf,
    )
    carried = cumulative + start_stable[..., None]
    running_max = jnp.maximum(carried, jnp.max(log_weight, axis=-1))
    scores = jnp.einsum("hctd,hcsd->hcts", query_block, key_blk, precision=HIGH) * jnp.exp(
        log_weight - running_max[..., None]
    )
    carry_weight = jnp.exp(carried - running_max)
    numerator = jnp.einsum("hcts,hcsv->hctv", scores, value_blk, precision=HIGH) + carry_weight[
        ..., None
    ] * jnp.einsum("hcvd,hctd->hctv", start_memory, query_block, precision=HIGH)
    denominator = jnp.sum(scores, axis=-1) + carry_weight * jnp.einsum(
        "hcd,hctd->hct", start_normer, query_block, precision=HIGH
    )
    result = numerator / jnp.maximum(jnp.abs(denominator), jnp.exp(-running_max))[..., None]
    return result.reshape(head_count, length, DV)


def flipped(source):
    return jnp.flip(source, axis=1)


def lstm_branch(
    normed,
    query_proj,
    key_proj,
    value_proj,
    w_gates,
    input_bias,
    forget_bias,
    decay_shift,
    head_gain,
):
    length = normed.shape[0]
    head_count = w_gates.shape[-1]
    gate_pre = jnp.dot(
        normed,
        w_gates.reshape(w_gates.shape[0], 4 * head_count),
        preferred_element_type=jnp.float32,
    ).reshape(length, 2, 2, head_count)
    queries = to_heads(query_proj, head_count) * DQK ** (-0.5)
    keys_all = to_heads(key_proj, head_count)
    values_all = to_heads(value_proj, head_count)
    summed = jnp.zeros((head_count, length, DV), jnp.float32)
    for direction in range(2):
        in_gate = (gate_pre[:, direction, 0, :] + input_bias[direction]).T
        log_forget = (
            jax.nn.log_sigmoid(gate_pre[:, direction, 1, :] + forget_bias[direction])
            + decay_shift[direction]
        ).T
        if direction == 1:
            result = flipped(
                local_pass(
                    flipped(queries),
                    flipped(keys_all),
                    flipped(values_all),
                    flipped(in_gate),
                    flipped(log_forget),
                    True,
                )
            )
        else:
            result = local_pass(queries, keys_all, values_all, in_gate, log_forget, False)
        summed = summed + result
    inverse_rms = lax.rsqrt(jnp.mean(summed * summed, axis=-1, keepdims=True) + EPS)
    return ((summed * inverse_rms).transpose(1, 0, 2) * head_gain.reshape(head_count, DV)).astype(
        jnp.bfloat16
    )


def conv_branch(gate_outer, gate_inner, conv_input, conv_taps):
    length = gate_outer.shape[0]
    mixed_in = (gate_inner.astype(jnp.float32) * conv_input.astype(jnp.float32)).astype(
        jnp.bfloat16
    )
    padded = padded_2(mixed_in, (("sp", 0),), 1).astype(jnp.float32)
    taps_wide = conv_taps.astype(jnp.float32)
    filtered = taps_wide[0] * padded[:-2] + taps_wide[1] * padded[1:-1] + taps_wide[2] * padded[2:]
    return (gate_outer.astype(jnp.float32) * filtered).astype(jnp.bfloat16).reshape(length, -1, DV)


def projected(normed, matrices):
    return tuple(
        (
            jnp.dot(normed, matrix, preferred_element_type=jnp.float32).astype(jnp.bfloat16)
            for matrix in matrices
        )
    )


def body(
    tokens,
    norm_gain,
    w_query,
    w_key,
    w_value,
    w_gates,
    input_bias,
    forget_bias,
    decay_shift,
    head_gain,
    w_conv_b,
    w_conv_c,
    w_conv_in,
    conv_taps,
    w_out,
):
    normed = row_norm(tokens, norm_gain)
    length = normed.shape[0]
    whole_mats = (
        lax.all_gather(w_query, "sp", axis=0, tiled=True),
        lax.all_gather(w_key, "sp", axis=0, tiled=True),
        lax.all_gather(w_value, "sp", axis=0, tiled=True),
        lax.all_gather(w_conv_b, "sp", axis=0, tiled=True),
        lax.all_gather(w_conv_c, "sp", axis=0, tiled=True),
        lax.all_gather(w_conv_in, "sp", axis=0, tiled=True),
    )
    query_proj, key_proj, value_proj, gate_outer, gate_inner, conv_input = projected(
        normed, whole_mats
    )
    lstm_out = lstm_branch(
        normed,
        query_proj,
        key_proj,
        value_proj,
        w_gates,
        input_bias,
        forget_bias,
        decay_shift,
        head_gain,
    )
    conv_out = conv_branch(gate_outer, gate_inner, conv_input, conv_taps)
    joined = jnp.stack([lstm_out, conv_out], axis=2).reshape(length, -1)
    joined_all = lax.all_gather(joined, "tp", axis=1, tiled=True)
    out_whole = lax.all_gather(w_out, "sp", axis=0, tiled=True)
    return jnp.dot(joined_all, out_whole, preferred_element_type=jnp.float32).astype(jnp.bfloat16)


def solution(mesh):
    placed = (
        P("sp", None),
        P(),
        P("sp", "tp"),
        P("sp", "tp"),
        P("sp", "tp"),
        P(None, None, None, "tp"),
        P(None, "tp"),
        P(None, "tp"),
        P(None, "sp", "tp"),
        P("tp"),
        P("sp", "tp"),
        P("sp", "tp"),
        P("sp", "tp"),
        P(None, "tp"),
        P("sp", "tp"),
    )
    return jax.shard_map(body, mesh=mesh, in_specs=placed, out_specs=P("sp", "tp"), check_vma=False)
```

profile of v0, /device:TPU:0, one launch (start us, length us, event | category | flops | bytes accessed | tf_op | source)
XLA Modules:
  0.0 511.0 jit_solution(5849541648931565221)
XLA Ops:
  6.6 0.7 all-gather.17.cloned.1.call-update
  7.3 0.7 all-gather.15.cloned.1.call-update
  8.1 0.7 all-gather.19.cloned.1.call-update
  10.6 2.1 fusion.8
  13.9 2.2 fusion.10
  16.8 1.4 fusion.62
  20.9 1.9 fusion.66
  23.6 3.6 fusion.84
  27.1 1.3 dynamic-update-slice.1
  29.5 1.9 fusion.65
  32.9 3.7 fusion.87
  36.6 1.3 dynamic-update-slice.3
  37.9 23.7 %all-reduce.8 = (f32[8]{0:T(128)}, f32[8]{0:T(128)}, f32[8]{0:T(128)S(1)}, f32[8]{0:T(128)S(1)}) all-reduce(f32[8]{0:T(128)S(1)} %fusion.66, f32[8]{0:T(128)S(1)} %dynamic-update-slice.1, f32[8]{0:T(128)S(1)} %fusion.65, f32[8]{0:T(128)S(1)} %dynamic-update-slice.3), channel_id=2, replica_groups=mesh['sp'=8,'tp'=4] {'sp'}, use_global_device_ids=true, to_apply=%add.4 | all-reduce | flops 32 | bytes 256
  63.0 1.7 fusion.85
  68.6 1.8 fusion.88
  73.2 0.7 reverse.17
  73.8 0.7 reverse.18
  74.7 0.8 select_reduce_fusion
  76.3 1.9 convolution_convert_fusion.5
  78.7 15.1 %all-gather.15.cloned.1.call-done = bf16[4096,128]{1,0:T(8,128)(2,1)} async-done(((bf16[512,128]{1,0:T(8,128)(2,1)}), bf16[4096,128]{1,0:T(8,128)(2,1)}) %all-gather.15.cloned.1.call-update) | async-done | bytes 1048592 | tf_op jit(solution)/shard_map/all_gather | solution.py:228
  93.8 2.6 broadcast_multiply_fusion.1
  96.4 47.4 %all-gather.19.cloned.1.call-done = bf16[4096,256]{1,0:T(8,128)(2,1)} async-done(((bf16[512,256]{1,0:T(8,128)(2,1)}), bf16[4096,256]{1,0:T(8,128)(2,1)}) %all-gather.19.cloned.1.call-update) | async-done | bytes 2097168 | tf_op jit(solution)/shard_map/all_gather | solution.py:230
  143.8 2.3 fusion.83
  146.5 0.8 fusion.46
  147.8 18.2 %all_gather.78 = f32[8,1,128]{2,1,0:T(1,128)S(1)} all-gather(f32[1,1,128]{2,1,0:T(1,128)S(1)} %get-tuple-element.431), channel_id=1, replica_groups=mesh['sp'=8,'tp'=4] {'sp'}, dimensions={0}, use_global_device_ids=true | all-gather | bytes 4608 | tf_op jit(solution)/shard_map/all_gather | solution.py:18
  167.1 17.2 %all_gather.72 = f32[8,1,128]{2,1,0:T(1,128)} all-gather(f32[1,1,128]{2,1,0:T(1,128)S(1)} %get-tuple-element.439), channel_id=1, replica_groups=mesh['sp'=8,'tp'=4] {'sp'}, dimensions={0}, use_global_device_ids=true | all-gather | bytes 4608 | tf_op jit(solution)/shard_map/all_gather | solution.py:18
  184.5 9.1 %all-gather.27.cloned.1.call-done = bf16[4096,256]{1,0:T(8,128)(2,1)} async-done(((bf16[512,256]{1,0:T(8,128)(2,1)}), bf16[4096,256]{1,0:T(8,128)(2,1)}) %all-gather.27.cloned.1.call-update) | async-done | bytes 2097168 | tf_op jit(solution)/shard_map/all_gather | solution.py:232
  193.7 2.5 fusion.20
  196.2 47.1 %all-gather.29.cloned.1.call-done = bf16[4096,256]{1,0:T(8,128)(2,1)} async-done(((bf16[512,256]{1,0:T(8,128)(2,1)}), bf16[4096,256]{1,0:T(8,128)(2,1)}) %all-gather.29.cloned.1.call-update) | async-done | bytes 2097168 | tf_op jit(solution)/shard_map/all_gather | solution.py:233
  243.3 2.5 fusion.19
  245.9 2.5 collective-permute-start
  248.4 1.3 collective-permute-start.1
  249.7 0.7 convolution_bitcast_fusion
  250.3 0.8 fusion.44
  252.0 3.9 collective-permute-done.1
  255.9 1.0 maximum_convert_fusion
  256.9 36.2 %all-gather.25.cloned.1.call-done = bf16[4096,256]{1,0:T(8,128)(2,1)} async-done(((bf16[512,256]{1,0:T(8,128)(2,1)}), bf16[4096,256]{1,0:T(8,128)(2,1)}) %all-gather.25.cloned.1.call-update) | async-done | bytes 2097168 | tf_op jit(solution)/shard_map/all_gather | solution.py:231
  293.1 3.3 fusion.24
  296.3 37.7 %all-gather.21.cloned.1.call-done = f32[8,1,256,128]{3,2,1,0:T(8,128)} async-done(((f32[1,1,256,128]{3,2,1,0:T(8,128)}), f32[8,1,256,128]{3,2,1,0:T(8,128)}) %all-gather.21.cloned.1.call-update) | async-done | bytes 1048592 | tf_op jit(solution)/shard_map/all_gather | solution.py:18
  334.1 29.4 %while.36 = (s32[]{:T(128)}, f32[1,256,128]{2,1,0:T(8,128)S(1)}, f32[1,128]{1,0:T(1,128)S(1)}, f32[1]{0:T(128)}, s32[]{:T(128)}, /*index=5*/f32[8,1]{0,1:T(1,128...) while((s32[]{:T(128)}, f32[1,256,128]{2,1,0:T(8,128)S(1)}, ...), condition=%wide.region_4.5_spmd.clone, body=%wide.region_3.4_spmd.clone.sunk | while | flops 164489 | bytes 395004 | solution.py:30
  336.6 1.0 fusion.133
  340.8 1.0 fusion.133
  345.0 1.0 fusion.133
  349.2 1.0 fusion.133
  353.3 1.0 fusion.133
  354.3 0.7 broadcast_select_fusion.6
  357.5 1.0 fusion.133
  358.5 0.7 broadcast_select_fusion.6
  361.8 1.0 fusion.133
  362.8 0.7 broadcast_select_fusion.6
  363.5 11.7 %all-gather.23.cloned.1.call-done = f32[8,1,256,128]{3,2,1,0:T(8,128)} async-done(((f32[1,1,256,128]{3,2,1,0:T(8,128)}), f32[8,1,256,128]{3,2,1,0:T(8,128)}) %all-gather.23.cloned.1.call-update) | async-done | bytes 1048592 | tf_op jit(solution)/shard_map/all_gather | solution.py:18
  375.2 1.3 rev.34
  376.6 23.4 %while.37 = (s32[]{:T(128)}, f32[1,256,128]{2,1,0:T(8,128)S(1)}, f32[1,128]{1,0:T(1,128)S(1)}, f32[1]{0:T(128)}, s32[]{:T(128)}, /*index=5*/f32[8,1]{0,1:T(1,128...) while((s32[]{:T(128)}, f32[1,256,128]{2,1,0:T(8,128)S(1)}, ...), condition=%wide.region_10.11_spmd.clone, body=%wide.region_9.10_spmd.clone.sunk | while | flops 164489 | bytes 395004 | solution.py:30
  376.6 0.7 constant_dynamic-slice_fusion.9
  379.3 0.7 broadcast_select_fusion.7
  392.6 0.7 broadcast_select_fusion.7
  399.3 0.7 broadcast_select_fusion.7
  400.0 1.3 subtract_exponential_fusion.7
  401.3 1.4 subtract_exponential_fusion.5
  402.7 1.4 subtract_exponential_fusion.4
  408.5 0.7 pad_maximum_fusion
  409.9 15.0 %all-gather.31.cloned.1.call-done = bf16[256,2048]{0,1:T(8,128)(2,1)} async-done(((bf16[256,512]{0,1:T(8,128)(2,1)}), bf16[256,2048]{0,1:T(8,128)(2,1)}) %all-gather.31.cloned.1.call-update) | async-done | bytes 1048592 | tf_op jit(solution)/shard_map/all_gather | solution.py:251
  424.8 74.8 %all-gather.33.cloned.1.call-done = bf16[2048,1024]{1,0:T(8,128)(2,1)} async-done(((bf16[256,1024]{1,0:T(8,128)(2,1)}), bf16[2048,1024]{1,0:T(8,128)(2,1)}) %all-gather.33.cloned.1.call-update) | async-done | bytes 4194320 | tf_op jit(solution)/shard_map/all_gather | solution.py:252
  499.6 4.6 convolution_convert_fusion
  (181 shorter events, 32.8 us)
Async XLA Ops:
  6.5 6.1 %copy-start.11 = (bf16[4096,2,2,1]{0,2,3,1:T(2,128)(2,1)S(1)}, bf16[4096,2,2,1]{0,2,3,1:T(2,128)(2,1)}, u32[]{:S(2)}) copy-start(bf16[4096,2,2,1]{0,2,3,1:T(2,128)(2,1)} %param.24) | copy-start | bytes 98308
  6.5 6.2 %copy-start.27 = (f32[2,1]{0,1:T(1,128)S(1)}, f32[2,1]{0,1:T(1,128)}, u32[]{:S(2)}) copy-start(f32[2,1]{0,1:T(1,128)} %param.26) | copy-start | bytes 28
  6.5 6.8 %copy-start.28 = (f32[2,1]{0,1:T(1,128)S(1)}, f32[2,1]{0,1:T(1,128)}, u32[]{:S(2)}) copy-start(f32[2,1]{0,1:T(1,128)} %param.25) | copy-start | bytes 28
  6.5 7.4 %copy-start.16 = (f32[4096]{0:T(1024)S(1)}, f32[4096]{0:T(1024)}, u32[]{:S(2)}) copy-start(f32[4096]{0:T(1024)} %param.20) | copy-start | bytes 49156
  6.5 69.7 %all-gather.17.cloned.1.call-start = ((), (), s32[]{:S(2)}) async-start(), calls=%async_computation.1 | async-start | bytes 1179648 | tf_op jit(solution)/shard_map/all_gather | solution.py:229
  7.3 86.5 %all-gather.15.cloned.1.call-start = ((), (), s32[]{:S(2)}) async-start(), calls=%async_computation | async-start | bytes 1179648 | tf_op jit(solution)/shard_map/all_gather | solution.py:228
  8.0 135.7 %all-gather.19.cloned.1.call-start = ((), (), s32[]{:S(2)}) async-start(), calls=%async_computation.2 | async-start | bytes 2359296 | tf_op jit(solution)/shard_map/all_gather | solution.py:230
  8.8 184.9 %all-gather.27.cloned.1.call-start = ((), (), s32[]{:S(2)}) async-start(), calls=%async_computation.6 | async-start | bytes 2359296 | tf_op jit(solution)/shard_map/all_gather | solution.py:232
  9.3 233.9 %all-gather.29.cloned.1.call-start = ((), (), s32[]{:S(2)}) async-start(), calls=%async_computation.7 | async-start | bytes 2359296 | tf_op jit(solution)/shard_map/all_gather | solution.py:233
  9.9 283.2 %all-gather.25.cloned.1.call-start = ((), (), s32[]{:S(2)}) async-start(), calls=%async_computation.5 | async-start | bytes 2359296 | tf_op jit(solution)/shard_map/all_gather | solution.py:231
  10.5 323.5 %all-gather.21.cloned.1.call-start = ((), (), s32[]{:S(2)}) async-start(), calls=%async_computation.3 | async-start | bytes 1179648 | tf_op jit(solution)/shard_map/all_gather | solution.py:18
  16.1 2.1 slice-start
  16.2 2.6 copy-start.26
  16.2 3.6 copy-start.32
  16.2 59.4 %copy-start.23 = (bf16[3,256]{1,0:T(4,128)(2,1)S(1)}, bf16[3,256]{1,0:T(4,128)(2,1)}, u32[]{:S(2)}) copy-start(bf16[3,256]{1,0:T(4,128)(2,1)} %param.32) | copy-start | bytes 4612
  18.2 58.0 %copy-start.17 = (f32[256,1,1,1]{0,2,1,3:T(1,128)}, f32[256,1,1,1]{0,2,1,3:T(1,128)S(1)}, u32[]{:S(2)}) copy-start(f32[256,1,1,1]{0,2,1,3:T(1,128)S(1)} %get-tuple-element.451) | copy-start | bytes 3076
  18.6 57.7 %copy-start.9 = (f32[1,2,128]{2,1,0:T(2,128)}, f32[1,2,128]{2,1,0:T(2,128)S(1)}, u32[]{:S(2)}) copy-start(f32[1,2,128]{2,1,0:T(2,128)S(1)} %reduce_window_sum.17) | copy-start | bytes 3076
  28.8 47.5 %copy-start.6 = (f32[1,2,128]{2,1,0:T(2,128)}, f32[1,2,128]{2,1,0:T(2,128)S(1)}, u32[]{:S(2)}) copy-start(f32[1,2,128]{2,1,0:T(2,128)S(1)} %reduce_window_sum.18) | copy-start | bytes 3076
  32.0 44.2 %copy-start.12 = (f32[1,256]{1,0:T(1,128)}, f32[1,256]{1,0:T(1,128)S(1)}, u32[]{:S(2)}) copy-start(f32[1,256]{1,0:T(1,128)S(1)} %broadcast_add_fusion) | copy-start | bytes 3076
  78.2 68.0 %copy-start = (bf16[256,128]{1,0:T(8,128)(2,1)}, bf16[256,128]{1,0:T(8,128)(2,1)S(1)}, u32[]{:S(2)}) copy-start(bf16[256,128]{1,0:T(8,128)(2,1)S(1)} %convolution_convert_fusion.5) | copy-start | bytes 196612
  147.2 228.0 %all-gather.23.cloned.1.call-start = ((), (), s32[]{:S(2)}) async-start(), calls=%async_computation.4 | async-start | bytes 1179648 | tf_op jit(solution)/shard_map/all_gather | solution.py:18
  245.9 5.4 %collective-permute-start = (bf16[1,256]{0,1:T(8,128)(2,1)S(1)}, bf16[1,256]{0,1:T(8,128)(2,1)S(1)}, u32[]{:S(2)}, u32[]{:S(2)}) collective-permute-start(bf16[1,256]{0,1:T(8,128)(2,1)S(1)} %get-tuple-element.447), channel_id=1, source_target_pairs={{0,4},{4,8},{8,12},{12,16},{16,20},{20,24},{24,28},{1,5},{5,9},{9,... | collective-permute-start | bytes 1544 | tf_op jit(solution)/shard_map/ppermute | solution.py:40
  248.4 7.5 %collective-permute-start.1 = (bf16[1,256]{0,1:T(8,128)(2,1)S(1)}, bf16[1,256]{0,1:T(8,128)(2,1)}, u32[]{:S(2)}, u32[]{:S(2)}) collective-permute-start(bf16[1,256]{0,1:T(8,128)(2,1)S(1)} %get-tuple-element.448), channel_id=1, source_target_pairs={{4,0},{8,4},{12,8},{16,12},{20,16},{24,20},{28,24},{5,1},{9,5},{13... | collective-permute-start | bytes 1544 | tf_op jit(solution)/shard_map/ppermute | solution.py:41
  251.1 173.7 %all-gather.31.cloned.1.call-start = ((), (), s32[]{:S(2)}) async-start(), calls=%async_computation.8 | async-start | bytes 1310720 | tf_op jit(solution)/shard_map/all_gather | solution.py:251
  251.3 0.6 copy-start.8
  293.1 41.0 %copy-start.15 = (f32[1,128]{1,0:T(1,128)S(1)}, f32[1,128]{1,0:T(1,128)}, u32[]{:S(2)}) copy-start(f32[1,128]{1,0:T(1,128)} %custom-call.1) | copy-start | bytes 1540
  293.1 41.0 %copy-start.21 = (f32[8]{0:T(128)S(1)}, f32[8]{0:T(128)}, u32[]{:S(2)}) copy-start(f32[8]{0:T(128)} %get-tuple-element.421) | copy-start | bytes 100
  293.1 41.0 %copy-start.22 = (f32[8]{0:T(128)S(1)}, f32[8]{0:T(128)}, u32[]{:S(2)}) copy-start(f32[8]{0:T(128)} %get-tuple-element.422) | copy-start | bytes 100
  334.1 42.5 %copy-start.14 = (f32[1,128]{1,0:T(1,128)S(1)}, f32[1,128]{1,0:T(1,128)}, u32[]{:S(2)}) copy-start(f32[1,128]{1,0:T(1,128)} %custom-call.3) | copy-start | bytes 1540
  334.1 42.5 %copy-start.19 = (f32[8]{0:T(128)S(1)}, f32[8]{0:T(128)}, u32[]{:S(2)}) copy-start(f32[8]{0:T(128)} %reverse.17) | copy-start | bytes 100
  334.1 42.5 %copy-start.20 = (f32[8]{0:T(128)S(1)}, f32[8]{0:T(128)}, u32[]{:S(2)}) copy-start(f32[8]{0:T(128)} %reverse.18) | copy-start | bytes 100
  363.5 40.6 %copy-start.30 = (f32[1,1,128]{2,1,0:T(1,128)S(1)}, f32[1,1,128]{2,1,0:T(1,128)}, u32[]{:S(2)}) copy-start(f32[1,1,128]{2,1,0:T(1,128)} %get-tuple-element.432) | copy-start | bytes 1540
  363.5 41.0 %copy-start.7 = (f32[1,2,128]{2,1,0:T(2,128)S(1)}, f32[1,2,128]{2,1,0:T(2,128)}, u32[]{:S(2)}) copy-start(f32[1,2,128]{2,1,0:T(2,128)} %copy-done.6) | copy-start | bytes 3076
  363.5 41.0 %copy-start.10 = (f32[1,2,128]{2,1,0:T(2,128)S(1)}, f32[1,2,128]{2,1,0:T(2,128)}, u32[]{:S(2)}) copy-start(f32[1,2,128]{2,1,0:T(2,128)} %copy-done.9) | copy-start | bytes 3076
  363.5 41.0 %copy-start.24 = (f32[2,128]{1,0:T(2,128)S(1)}, f32[2,128]{1,0:T(2,128)}, u32[]{:S(2)}) copy-start(f32[2,128]{1,0:T(2,128)} %get-tuple-element.383) | copy-start | bytes 3076
  363.5 41.0 %copy-start.25 = (f32[2,128]{1,0:T(2,128)S(1)}, f32[2,128]{1,0:T(2,128)}, u32[]{:S(2)}) copy-start(f32[2,128]{1,0:T(2,128)} %get-tuple-element.384) | copy-start | bytes 3076
  363.5 41.1 %copy-start.13 = (f32[1,256]{1,0:T(1,128)S(1)}, f32[1,256]{1,0:T(1,128)}, u32[]{:S(2)}) copy-start(f32[1,256]{1,0:T(1,128)} %copy-done.12) | copy-start | bytes 3076
  376.5 29.0 %copy-start.5 = (f32[1,1,256,128]{3,2,1,0:T(8,128)S(1)}, f32[1,1,256,128]{3,2,1,0:T(8,128)}, u32[]{:S(2)}) copy-start(f32[1,1,256,128]{3,2,1,0:T(8,128)} %get-tuple-element.434) | copy-start | bytes 393220
  400.0 6.6 %copy-start.29 = (f32[1,1,128]{2,1,0:T(1,128)S(1)}, f32[1,1,128]{2,1,0:T(1,128)}, u32[]{:S(2)}) copy-start(f32[1,1,128]{2,1,0:T(1,128)} %get-tuple-element.440) | copy-start | bytes 1540
  400.0 6.7 %copy-start.3 = (f32[256,128]{1,0:T(8,128)S(1)}, f32[256,128]{1,0:T(8,128)}, u32[]{:S(2)}) copy-start(f32[256,128]{1,0:T(8,128)} %get-tuple-element.467) | copy-start | bytes 393220
  400.0 7.0 %copy-start.1 = (bf16[256,128]{1,0:T(8,128)(2,1)S(1)}, bf16[256,128]{1,0:T(8,128)(2,1)}, u32[]{:S(2)}) copy-start(bf16[256,128]{1,0:T(8,128)(2,1)} %copy-done) | copy-start | bytes 196612
  400.0 7.0 %copy-start.18 = (f32[256,1,1,1]{0,2,1,3:T(1,128)S(1)}, f32[256,1,1,1]{0,2,1,3:T(1,128)}, u32[]{:S(2)}) copy-start(f32[256,1,1,1]{0,2,1,3:T(1,128)} %copy-done.17) | copy-start | bytes 3076
  405.0 2.7 copy-start.4
  406.2 2.2 copy-start.31
  406.5 2.0 copy-start.2
  409.3 90.4 %all-gather.33.cloned.1.call-start = ((), (), s32[]{:S(2)}) async-start(), calls=%async_computation.9 | async-start | bytes 4718592 | tf_op jit(solution)/shard_map/all_gather | solution.py:252
Sparse Core Ops, SparseCore 0:
  9.5 43.1 all-gather.16
  54.8 38.9 all-gather.14
  95.9 47.7 all-gather.18
  145.7 47.8 all-gather.26
  195.6 47.5 all-gather.28
  245.2 47.7 all-gather.24
  295.2 38.7 all-gather.20
  336.2 39.0 all-gather.22
  409.4 15.3 all-gather.30
  426.8 72.7 all-gather.32
where the time goes:
time: 513 us; the launch traced here: 511 us
  waiting for transfers between devices  302 us (59%)
  blocking collectives  59.1 us (12%)
  other arithmetic  48.9 us (10%)
  loops' own time  27.5 us (5%)
  matrix products  24.6 us (5%)
  local copies, waits for them, and re-layouts  22.3 us (4%)
  between operations  22.1 us (4%)
    all_gather x1, waiting for transfers between devices, body(): out_whole = lax.all_gather(w_out, 'sp', axis=0, tiled=True)  74.8 us
    all_gather x2, waiting for transfers between devices, carried_in(): pieces = jax.tree.map(lambda part: lax.all_gather(part, axis), value)  49.4 us
    all_gather x1, waiting for transfers between devices, body(): lax.all_gather(w_value, 'sp', axis=0, tiled=True)  47.4 us
    all_gather x1, waiting for transfers between devices, body(): lax.all_gather(w_conv_in, 'sp', axis=0, tiled=True)  47.1 us
    all_gather x1, waiting for transfers between devices, body(): lax.all_gather(w_conv_b, 'sp', axis=0, tiled=True)  36.2 us
    all_gather x2, blocking collectives, carried_in(): pieces = jax.tree.map(lambda part: lax.all_gather(part, axis), value)  35.4 us
    another operation x2, loops' own time, carried_in(): return lax.fori_loop(0, count - 1, lap, subtotal)  27.5 us
    unnamed x1, blocking collectives  23.7 us
  transfers between devices with their start and end apart: 12, of which 10 were waited for; matrix products, arithmetic and copies ran while one was open for 14% of the time, Pallas kernels for 0%

commit v1 on v0

v1 whole, which is shorter than its diff:
```python
import functools

import jax
import jax.numpy as jnp
from jax import lax
from jax.experimental import pallas as pl
from jax.experimental.pallas import tpu as pltpu
from jax.sharding import PartitionSpec as P

EPS = 1e-06
HIGH = lax.Precision.HIGHEST
LOWEST = -1e30
F32 = jnp.float32
BF16 = jnp.bfloat16


def dot(a, b, dims, precision=None):
    return lax.dot_general(a, b, (dims, ((), ())), precision=precision, preferred_element_type=F32)


NN = ((1,), (0,))
NT = ((1,), (1,))
TN = ((0,), (0,))


def ring_place(index, n):
    odd = lax.rem(index, 2)
    half = lax.div(index, 2)
    return (1 - odd) * half + odd * (n - 1 - half)


def ring_index(place, n):
    late = lax.div(place, n // 2)
    return (1 - late) * (2 * place) + late * (2 * (n - 1 - place) + 1)


def kernel(
    n,
    t,
    dk,
    dv,
    tokens,
    norm_gain,
    w_own,
    wo_own,
    w_gates,
    gate_bias,
    decay,
    head_gain,
    taps,
    out,
    normed,
    w_all,
    wo_all,
    proj,
    state_out,
    pack_out,
    state_in,
    pack_in,
    carry_c,
    carry_n,
    joined,
    w_ss,
    w_rs,
    wo_ss,
    wo_rs,
    st_ss,
    st_rs,
    pk_ss,
    pk_rs,
    j_ss,
    j_rs,
):
    me = lax.axis_index("sp")
    head = lax.axis_index("tp")
    place = ring_place(me, n)
    right = ring_index(lax.rem(place + 1, n), n)
    left = ring_index(lax.rem(place + n - 1, n), n)
    rows = tokens.shape[0]

    barrier = pltpu.get_barrier_semaphore()

    def greet_sp(o, c):
        pl.semaphore_signal(barrier, inc=1, device_id={"sp": lax.rem(me + o, n)})
        return c

    def greet_tp(o, c):
        pl.semaphore_signal(barrier, inc=1, device_id={"tp": lax.rem(head + o, t)})
        return c

    lax.fori_loop(1, n, greet_sp, 0)
    lax.fori_loop(1, t, greet_tp, 0)
    pl.semaphore_wait(barrier, n + t - 2)

    def hop(own, whole, ss, rs, way, step, first):
        depth, width = own.shape
        half = width // 2
        holder = ring_index(lax.rem(place + (n + step if way else n - step), n), n)
        columns = pl.ds(way * half, half)
        there = whole.at[pl.ds(pl.multiple_of(holder * depth, depth), depth), columns]
        return pltpu.make_async_remote_copy(
            src_ref=own.at[:, columns] if first else there,
            dst_ref=there,
            send_sem=ss.at[way, step],
            recv_sem=rs.at[way, step],
            device_id={"sp": left if way else right},
        )

    def ring_start(*ring):
        for way in range(2):
            hop(*ring, way, 0, True).start()

    def ring_step(step, *ring):
        for way in range(2):
            hop(*ring, way, step - 1, False).wait_recv()
            hop(*ring, way, step, False).start()

    def ring_end(*ring):
        for way in range(2):
            hop(*ring, way, n - 2, False).wait_recv()

        def drain(step, c):
            for way in range(2):
                hop(*ring, way, step, False).wait_send()
            return c

        lax.fori_loop(0, n - 1, drain, 0)

    w_ring = (w_own, w_all, w_ss, w_rs)
    wo_ring = (wo_own, wo_all, wo_ss, wo_rs)
    ring_start(*w_ring)

    depth = w_own.shape[0]
    w_all[pl.ds(pl.multiple_of(me * depth, depth), depth), :] = w_own[...]
    depth_o = wo_own.shape[0]
    wo_all[pl.ds(pl.multiple_of(me * depth_o, depth_o), depth_o), :] = wo_own[...]

    chunk = 32

    def norm_rows(i, c):
        span = pl.ds(pl.multiple_of(i * chunk, chunk), chunk)
        values = tokens[span, :].astype(F32)
        inverse = lax.rsqrt(jnp.mean(values * values, axis=-1, keepdims=True) + EPS)
        normed[span, :] = (values * inverse * norm_gain[...]).astype(BF16)
        return c

    lax.fori_loop(0, rows // chunk, norm_rows, 0)

    gates = dot(w_gates[...], normed[...], NT) + gate_bias[...]
    forget = jnp.minimum(gates, 0.0) - jnp.log1p(jnp.exp(-jnp.abs(gates))) + decay[...]
    row_id = lax.broadcasted_iota(jnp.int32, (rows, rows), 0)
    col_id = lax.broadcasted_iota(jnp.int32, (rows, rows), 1)
    upto = (row_id <= col_id).astype(F32)
    after = (row_id >= col_id).astype(F32)
    sums = (dot(forget, upto, NN, HIGH), dot(forget, after, NN, HIGH))
    gates_t = gates.T
    sums_t = (sums[0].T, sums[1].T)

    lax.fori_loop(1, n - 1, lambda s, c: (ring_step(s, *w_ring), c)[1], 0)
    ring_end(*w_ring)

    ring_start(*wo_ring)
    done = [0]

    def advance():
        if done[0] + 1 < n - 1:
            done[0] += 1
            ring_step(done[0], *wo_ring)

    width = 256

    def project(i, c):
        span = pl.ds(pl.multiple_of(i * width, width), width)
        proj[:, span] = dot(normed[...], w_all[:, span], NN).astype(BF16)
        return c

    lax.fori_loop(0, w_own.shape[1] // width, project, 0)

    query = proj[:, :dk]
    keys = proj[:, dk : 2 * dk]
    values = proj[:, 2 * dk : 2 * dk + dv]
    base = 2 * dk + dv
    bw = (proj.shape[1] - base) // 3
    mixed = (proj[:, base + bw : base + 2 * bw].astype(F32) * proj[:, base + 2 * bw :].astype(F32)).astype(BF16).astype(F32)

    keys_f = keys.astype(F32)
    totals = []
    for d in range(2):
        cum_c = sums_t[d][:, 2 + d : 3 + d]
        in_c = gates_t[:, d : d + 1]
        last = rows - 1 if d == 0 else 0
        total = cum_c[last : last + 1, :]
        update = total - cum_c + in_c
        stable = jnp.max(update, axis=0, keepdims=True)
        weighted = keys_f * jnp.exp(update - stable)
        state_out[d] = dot(weighted.astype(BF16), values, TN).astype(BF16)
        edge = mixed[rows - 1 :, :] if d == 0 else mixed[:1, :]
        wide = pack_out.shape[-1]
        pack_out[d, 0:1, :] = edge
        pack_out[d, 1:2, :dk] = jnp.sum(weighted, axis=0, keepdims=True)
        pack_out[d, 1:2, dk:] = jnp.zeros((1, wide - dk), F32)
        pack_out[d, 2:3, :] = jnp.broadcast_to(total, (1, wide))
        pack_out[d, 3:4, :] = jnp.broadcast_to(stable, (1, wide))
        pack_out[d, 4:, :] = jnp.zeros((4, wide), F32)

    def give(o):
        other = lax.rem(me + o, n)
        d = lax.div(me + o, n)
        ids = {"sp": other}
        return (
            pltpu.make_async_remote_copy(state_out.at[d], state_in.at[me], st_ss.at[o], st_rs.at[me], device_id=ids),
            pltpu.make_async_remote_copy(pack_out.at[d], pack_in.at[me], pk_ss.at[o], pk_rs.at[me], device_id=ids),
        )

    def take(o):
        source = lax.rem(me + o, n)
        ids = {"sp": source}
        return (
            pltpu.make_async_remote_copy(state_out.at[0], state_in.at[source], st_ss.at[o], st_rs.at[source], device_id=ids),
            pltpu.make_async_remote_copy(pack_out.at[0], pack_in.at[source], pk_ss.at[o], pk_rs.at[source], device_id=ids),
        )

    def give_all(o, c):
        for copy in give(o):
            copy.start()
        return c

    def take_all(o, c):
        for copy in take(o):
            copy.wait_recv()
        return c

    def give_end(o, c):
        for copy in give(o):
            copy.wait_send()
        return c

    lax.fori_loop(1, n, give_all, 0)
    advance()

    scale = dk ** (-0.5)
    scores = dot(query, keys, NT) * scale
    local = []
    for d in range(2):
        cum_c = sums_t[d][:, 2 + d : 3 + d]
        cum_r = sums[d][2 + d : 3 + d, :]
        in_r = gates[d : d + 1, :]
        allowed = row_id >= col_id if d == 0 else row_id <= col_id
        log_weight = jnp.where(allowed, cum_c - cum_r + in_r, -jnp.inf)
        peak = jnp.max(log_weight, axis=-1, keepdims=True)
        part = scores * jnp.exp(log_weight - peak)
        num = dot(part, values.astype(F32), NN, HIGH)
        local.append((cum_c, peak, num, jnp.sum(part, axis=-1, keepdims=True)))
        advance()

    lax.fori_loop(1, n, take_all, 0)

    before = pack_in[lax.rem(me + n - 1, n), 0:1, :] * jnp.minimum(me, 1).astype(F32)
    behind = pack_in[lax.rem(me + 1, n), 0:1, :] * jnp.minimum(n - 1 - me, 1).astype(F32)
    pos = lax.broadcasted_iota(jnp.int32, mixed.shape, 0)
    prior = jnp.where(pos == 0, before, pltpu.roll(mixed, 1, 0))
    later = jnp.where(pos == rows - 1, behind, pltpu.roll(mixed, rows - 1, 0))
    taps_f = taps[...].astype(F32)
    filtered = taps_f[0:1] * prior + taps_f[1:2] * mixed + taps_f[2:3] * later
    joined[head, :, dv:] = (proj[:, base : base + bw].astype(F32) * filtered).astype(BF16)

    def share(part, o, source):
        columns = pl.ds(part * dv, dv)
        slot = joined.at[source, :, columns]
        return pltpu.make_async_remote_copy(
            slot,
            slot,
            j_ss.at[part, o],
            j_rs.at[part, source],
            device_id={"tp": lax.rem(head + o, t)},
        )

    for o in range(1, t):
        share(1, o, head).start()
    advance()

    summed = None
    query_f = query.astype(F32) * scale
    for d in range(2):
        carry_c[...] = jnp.zeros_like(carry_c)
        carry_n[...] = jnp.zeros_like(carry_n)

        def join(i, peak_in):
            source = i if d == 0 else n - 1 - i
            total = pack_in[source, 2:3, :]
            stable = pack_in[source, 3:4, :]
            new = jnp.maximum(peak_in + total, stable)
            old_w = jnp.exp(peak_in + total - new)
            new_w = jnp.exp(stable - new)
            carry_c[...] = old_w * carry_c[...] + new_w * state_in[source].astype(F32)
            carry_n[...] = old_w * carry_n[...] + new_w * pack_in[source, 1:2, :]
            return new

        peak_in = lax.fori_loop(0, me if d == 0 else n - 1 - me, join, jnp.full((1, dv), LOWEST, F32))
        cum_c, peak, num, den = local[d]
        carried = cum_c + peak_in[:, :1]
        top = jnp.maximum(carried, peak)
        carry_w = jnp.exp(carried - top)
        own_w = jnp.exp(peak - top)
        num = own_w * num + carry_w * dot(query_f, carry_c[...], NN, HIGH)
        den = own_w * den + carry_w * jnp.sum(query_f * carry_n[:, :dk], axis=-1, keepdims=True)
        result = num / jnp.maximum(jnp.abs(den), jnp.exp(-top))
        summed = result if d == 0 else summed + result
        advance()
    inverse = lax.rsqrt(jnp.mean(summed * summed, axis=-1, keepdims=True) + EPS)
    joined[head, :, :dv] = (summed * inverse * head_gain[...]).astype(BF16)
    for o in range(1, t):
        share(0, o, head).start()

    lax.fori_loop(done[0] + 1, n - 1, lambda s, c: (ring_step(s, *wo_ring), c)[1], 0)
    ring_end(*wo_ring)
    for part in range(2):
        for o in range(1, t):
            share(part, o, lax.rem(head + o, t)).wait_recv()

    span_j = 2 * dv

    def emit(i, c):
        span = pl.ds(pl.multiple_of(i * width, width), width)
        total = dot(joined[0], wo_all[0:span_j, span], NN)
        for j in range(1, t):
            total += dot(joined[j], wo_all[j * span_j : (j + 1) * span_j, span], NN)
        out[:, span] = total.astype(BF16)
        return c

    lax.fori_loop(0, out.shape[1] // width, emit, 0)
    lax.fori_loop(1, n, give_end, 0)
    for part in range(2):
        for o in range(1, t):
            share(part, o, head).wait_send()


def body(
    n,
    t,
    tokens,
    norm_gain,
    w_query,
    w_key,
    w_value,
    w_gates,
    input_bias,
    forget_bias,
    decay_shift,
    head_gain,
    w_conv_b,
    w_conv_c,
    w_conv_in,
    conv_taps,
    w_out,
):
    rows, model = tokens.shape
    dk, dv = w_query.shape[1], w_value.shape[1]
    w_own = jnp.concatenate([w_query, w_key, w_value, w_conv_b, w_conv_c, w_conv_in], axis=1)
    gates = jnp.transpose(w_gates[..., 0], (2, 1, 0)).reshape(4, model)
    gates = jnp.pad(gates, ((0, 4), (0, 0)))
    bias = jnp.concatenate([input_bias, forget_bias, jnp.zeros((4, 1), F32)], axis=0)
    decay = jnp.pad(decay_shift[..., 0], ((2, 4), (0, 0)))
    wide, cols = w_own.shape[1], w_out.shape[1]
    vmem = pl.BlockSpec(memory_space=pltpu.VMEM)
    dma = pltpu.SemaphoreType.DMA
    return pl.pallas_call(
        functools.partial(kernel, n, t, dk, dv),
        out_shape=jax.ShapeDtypeStruct((rows, cols), BF16),
        in_specs=[vmem] * 9,
        out_specs=vmem,
        scratch_shapes=[
            pltpu.VMEM((rows, model), BF16),
            pltpu.VMEM((n * w_own.shape[0], wide), BF16),
            pltpu.VMEM((n * w_out.shape[0], cols), BF16),
            pltpu.VMEM((rows, wide), BF16),
            pltpu.VMEM((2, dk, dv), BF16),
            pltpu.VMEM((2, 8, dv), F32),
            pltpu.VMEM((n, dk, dv), BF16),
            pltpu.VMEM((n, 8, dv), F32),
            pltpu.VMEM((dk, dv), F32),
            pltpu.VMEM((1, dv), F32),
            pltpu.VMEM((t, rows, 2 * dv), BF16),
            dma((2, n - 1)),
            dma((2, n - 1)),
            dma((2, n - 1)),
            dma((2, n - 1)),
            dma((n,)),
            dma((n,)),
            dma((n,)),
            dma((n,)),
            dma((2, t)),
            dma((2, t)),
        ],
        compiler_params=pltpu.CompilerParams(
            collective_id=0, has_side_effects=True, vmem_limit_bytes=60 * 1024 * 1024
        ),
    )(
        tokens,
        norm_gain.reshape(1, model),
        w_own,
        w_out,
        gates,
        bias,
        decay,
        head_gain.reshape(1, dv),
        conv_taps,
    )


def solution(mesh):
    placed = (
        P("sp", None),
        P(),
        P("sp", "tp"),
        P("sp", "tp"),
        P("sp", "tp"),
        P(None, None, None, "tp"),
        P(None, "tp"),
        P(None, "tp"),
        P(None, "sp", "tp"),
        P("tp"),
        P("sp", "tp"),
        P("sp", "tp"),
        P("sp", "tp"),
        P(None, "tp"),
        P("sp", "tp"),
    )
    step = functools.partial(body, mesh.shape["sp"], mesh.shape["tp"])
    return jax.shard_map(step, mesh=mesh, in_specs=placed, out_specs=P("sp", "tp"), check_vma=False)
```

time: 513 us -> 182 us (0.35)
  waiting for transfers between devices: 302 us -> 0 us
  Pallas kernels: 0 us -> 173 us
  blocking collectives: 59.1 us -> 0 us
  other arithmetic: 48.9 us -> 0.07 us
  loops' own time: 27.5 us -> 0 us
  matrix products: 24.6 us -> 0 us
  between operations: 22.1 us -> 0.11 us
  local copies, waits for them, and re-layouts: 22.3 us -> 7.93 us
    all_gather x10 -> x0, waiting for transfers between devices: 294 us -> none  [the longest x1 74.8 us: body(): out_whole = lax.all_gather(w_out, 'sp', axis=0, tiled=True)]
    pallas_call x0 -> x1, Pallas kernels: none -> 173 us  [body(): pl.pallas_call(functools.partial(kernel, n, t, dk, dv), out_shape=jax.Sha...]
    all_gather x2 -> x0, blocking collectives: 35.4 us -> none  [carried_in(): pieces = jax.tree.map(lambda part: lax.all_gather(part, axis), value)]
    another operation x2 -> x0, loops' own time: 27.5 us -> none  [carried_in(): return lax.fori_loop(0, count - 1, lap, subtotal)]
    dot_general x20 -> x0, matrix products: 24.6 us -> none  [the longest x6 15.1 us: projected(): jnp.dot(normed, matrix, preferred_element_type=jnp.float32)]
    unnamed x1 -> x0, blocking collectives: 23.7 us -> none
    select_n x28 -> x0, other arithmetic: 16.5 us -> none  [lap(): jnp.where(position < mine, new, old)]
    sub x4 -> x0, other arithmetic: 10.9 us -> none  [the longest x2 7.31 us: combine(): weight_b = jnp.exp(stable_b - stable)]
  transfers between devices with their start and end apart: 12 -> 0, of which waited for: 10 -> 0; matrix products, arithmetic and copies ran while one was open for 14% -> 0% of each run, Pallas kernels for 0% -> 0%
where the time goes in v1:
time: 182 us; the launch traced here: 181 us
  Pallas kernels  173 us (95%)
  local copies, waits for them, and re-layouts  7.93 us (4%)
    pallas_call x1, Pallas kernels, body(): pl.pallas_call(functools.partial(kernel, n, t, dk, dv), out_shape=jax.Sha...  173 us
    unnamed x21, local copies, waits for them, and re-layouts  5.8 us

profile of v1, /device:TPU:0, one launch (start us, length us, event | category | flops | bytes accessed | tf_op | source)
XLA Modules:
  0.0 181.4 jit_solution(7657018626103443897)
XLA Ops:
  0.0 0.0 copy-start.1
  0.0 0.0 copy-start.2
  0.0 0.0 copy-start.3
  0.0 1.0 constant_dynamic-update-slice_fusion.5
  1.0 0.0 copy-start.4
  1.0 0.0 copy-start.5
  1.0 0.0 copy-start.6
  1.0 0.9 constant_dynamic-update-slice_fusion.4
  2.0 1.0 constant_dynamic-update-slice_fusion.3
  3.0 1.0 constant_dynamic-update-slice_fusion.2
  3.9 0.0 copy-done.1
  4.0 0.0 copy-done.2
  4.0 0.0 copy-start
  4.0 0.0 copy-done.3
  4.1 0.8 pad.8.w_gates
  4.9 0.0 copy-done.4
  4.9 0.6 pad.9.decay
  5.5 0.0 copy-done.5
  5.5 0.0 copy-done.6
  5.5 0.1 bitcast_maximum_fusion
  5.6 0.7 copy.20.gate_bias
  6.2 0.0 copy-done
  6.2 173.3 %shard_map.145 = bf16[256,1024]{1,0:T(8,128)(2,1)} custom-call(bf16[256,4096]{1,0:T(8,128)(2,1)} %tokens.1, f32[1,4096]{1,0:T(1,128)} %bitcast.11, bf16[512,1280]{1,0:T(8,128)(2,1)} %copy-done, bf16[256,1024]{1,0:T(8,128)(2,1)} %wo_own.1, bf16[8,4096]{1,0:T(8,128)(2,1)} %pad.8.w_gates, f32[8,1]{1,0:T(8,128)} %copy.20.gate_bias, f32[8,256]{1,0:T(8,128)} %pad.9.decay, ...), custom_call_target="tpu_custom_call" | custom-call | tf_op jit(solution)/shard_map/pallas_call | solution.py:367
  179.6 1.9 %copy.30 = bf16[256,1024]{1,0:T(8,128)(2,1)} copy(bf16[256,1024]{1,0:T(8,128)(2,1)} %shard_map.145) | data formatting | bytes 1048576
  (6 shorter events, 0.1 us)
Async XLA Ops:
  0.0 3.9 %copy-start.1 = (bf16[512,256]{1,0:T(8,128)(2,1)S(1)}, bf16[512,256]{1,0:T(8,128)(2,1)}, u32[]{:S(2)}) copy-start(bf16[512,256]{1,0:T(8,128)(2,1)} %param.26) | copy-start | bytes 786436
  0.0 4.0 %copy-start.2 = (bf16[512,256]{1,0:T(8,128)(2,1)S(1)}, bf16[512,256]{1,0:T(8,128)(2,1)}, u32[]{:S(2)}) copy-start(bf16[512,256]{1,0:T(8,128)(2,1)} %param.27) | copy-start | bytes 786436
  0.0 4.0 %copy-start.3 = (bf16[4096,2,2,1]{0,2,3,1:T(2,128)(2,1)S(1)}, bf16[4096,2,2,1]{0,2,3,1:T(2,128)(2,1)}, u32[]{:S(2)}) copy-start(bf16[4096,2,2,1]{0,2,3,1:T(2,128)(2,1)} %param.20) | copy-start | bytes 98308
  1.0 3.9 %copy-start.4 = (f32[2,256,1]{1,2,0:T(1,128)S(1)}, f32[2,256,1]{1,2,0:T(1,128)}, u32[]{:S(2)}) copy-start(f32[2,256,1]{1,2,0:T(1,128)} %param.23) | copy-start | bytes 6148
  1.0 4.5 %copy-start.5 = (f32[2,1]{0,1:T(1,128)S(1)}, f32[2,1]{0,1:T(1,128)}, u32[]{:S(2)}) copy-start(f32[2,1]{0,1:T(1,128)} %param.22) | copy-start | bytes 28
  1.0 4.5 %copy-start.6 = (f32[2,1]{0,1:T(1,128)S(1)}, f32[2,1]{0,1:T(1,128)}, u32[]{:S(2)}) copy-start(f32[2,1]{0,1:T(1,128)} %param.21) | copy-start | bytes 28
  4.0 2.2 %copy-start = (bf16[512,1280]{1,0:T(8,128)(2,1)}, bf16[512,1280]{1,0:T(8,128)(2,1)S(1)}, u32[]{:S(2)}) copy-start(bf16[512,1280]{1,0:T(8,128)(2,1)S(1)} %constant_dynamic-update-slice_fusion.w_own) | copy-start | bytes 3932164

commit v2 on v1

--- a/solution.py
+++ b/solution.py
@@ -10,6 +10,7 @@
 EPS = 1e-06
 HIGH = lax.Precision.HIGHEST
 LOWEST = -1e30
+PIECES = 4
 F32 = jnp.float32
 BF16 = jnp.bfloat16
 
@@ -32,6 +33,10 @@
 def ring_index(place, n):
     late = lax.div(place, n // 2)
     return (1 - late) * (2 * place) + late * (2 * (n - 1 - place) + 1)
+
+
+def pieces(own):
+    return max(1, min(PIECES, own.shape[0] // 16))
 
 
 def kernel(
@@ -92,36 +97,42 @@
     lax.fori_loop(1, t, greet_tp, 0)
     pl.semaphore_wait(barrier, n + t - 2)
 
-    def hop(own, whole, ss, rs, way, step, first):
+    def hop(own, whole, ss, rs, way, step, piece, first):
         depth, width = own.shape
-        half = width // 2
+        half, tall = width // 2, depth // pieces(own)
         holder = ring_index(lax.rem(place + (n + step if way else n - step), n), n)
         columns = pl.ds(way * half, half)
-        there = whole.at[pl.ds(pl.multiple_of(holder * depth, depth), depth), columns]
+        there = whole.at[pl.ds(pl.multiple_of(holder * depth + piece * tall, tall), tall), columns]
+        turn = step * pieces(own) + piece
         return pltpu.make_async_remote_copy(
-            src_ref=own.at[:, columns] if first else there,
+            src_ref=own.at[pl.ds(piece * tall, tall), columns] if first else there,
             dst_ref=there,
-            send_sem=ss.at[way, step],
-            recv_sem=rs.at[way, step],
+            send_sem=ss.at[way, turn],
+            recv_sem=rs.at[way, turn],
             device_id={"sp": left if way else right},
         )
 
     def ring_start(*ring):
-        for way in range(2):
-            hop(*ring, way, 0, True).start()
+        for piece in range(pieces(ring[0])):
+            for way in range(2):
+                hop(*ring, way, 0, piece, True).start()
 
     def ring_step(step, *ring):
-        for way in range(2):
-            hop(*ring, way, step - 1, False).wait_recv()
-            hop(*ring, way, step, False).start()
-
-    def ring_end(*ring):
-        for way in range(2):
-            hop(*ring, way, n - 2, False).wait_recv()
-
+        for piece in range(pieces(ring[0])):
+            for way in range(2):
+                hop(*ring, way, step - 1, piece, False).wait_recv()
+                hop(*ring, way, step, piece, False).start()
+
+    def ring_last(*ring):
+        for piece in range(pieces(ring[0])):
+            for way in range(2):
+                hop(*ring, way, n - 2, piece, False).wait_recv()
+
+    def ring_drain(*ring):
         def drain(step, c):
-            for way in range(2):
-                hop(*ring, way, step, False).wait_send()
+            for piece in range(pieces(ring[0])):
+                for way in range(2):
+                    hop(*ring, way, step, piece, False).wait_send()
             return c
 
         lax.fori_loop(0, n - 1, drain, 0)
@@ -157,9 +168,8 @@
     sums_t = (sums[0].T, sums[1].T)
 
     lax.fori_loop(1, n - 1, lambda s, c: (ring_step(s, *w_ring), c)[1], 0)
-    ring_end(*w_ring)
-
     ring_start(*wo_ring)
+    ring_last(*w_ring)
     done = [0]
 
     def advance():
@@ -306,14 +316,15 @@
         den = own_w * den + carry_w * jnp.sum(query_f * carry_n[:, :dk], axis=-1, keepdims=True)
         result = num / jnp.maximum(jnp.abs(den), jnp.exp(-top))
         summed = result if d == 0 else summed + result
-        advance()
+        if d == 0:
+            advance()
     inverse = lax.rsqrt(jnp.mean(summed * summed, axis=-1, keepdims=True) + EPS)
     joined[head, :, :dv] = (summed * inverse * head_gain[...]).astype(BF16)
     for o in range(1, t):
         share(0, o, head).start()
 
     lax.fori_loop(done[0] + 1, n - 1, lambda s, c: (ring_step(s, *wo_ring), c)[1], 0)
-    ring_end(*wo_ring)
+    ring_last(*wo_ring)
     for part in range(2):
         for o in range(1, t):
             share(part, o, lax.rem(head + o, t)).wait_recv()
@@ -329,6 +340,8 @@
         return c
 
     lax.fori_loop(0, out.shape[1] // width, emit, 0)
+    ring_drain(*w_ring)
+    ring_drain(*wo_ring)
     lax.fori_loop(1, n, give_end, 0)
     for part in range(2):
         for o in range(1, t):
@@ -381,10 +394,10 @@
             pltpu.VMEM((dk, dv), F32),
             pltpu.VMEM((1, dv), F32),
             pltpu.VMEM((t, rows, 2 * dv), BF16),
-            dma((2, n - 1)),
-            dma((2, n - 1)),
-            dma((2, n - 1)),
-            dma((2, n - 1)),
+            dma((2, (n - 1) * pieces(w_own))),
+            dma((2, (n - 1) * pieces(w_own))),
+            dma((2, (n - 1) * pieces(w_out))),
+            dma((2, (n - 1) * pieces(w_out))),
             dma((n,)),
             dma((n,)),
             dma((n,)),

time: 182 us -> 172 us (0.945)
  Pallas kernels: 173 us -> 164 us
    pallas_call x1, Pallas kernels: 173 us -> 164 us  [body(): pl.pallas_call(functools.partial(kernel, n, t, dk, dv), out_shape=jax.Sha...]
where the time goes in v2:
time: 172 us
  Pallas kernels  164 us (95%)
  local copies, waits for them, and re-layouts  7.93 us (5%)
    pallas_call x1, Pallas kernels, body(): pl.pallas_call(functools.partial(kernel, n, t, dk, dv), out_shape=jax.Sha...  164 us
    unnamed x21, local copies, waits for them, and re-layouts  5.8 us

profile of v2, /device:TPU:0, one launch (start us, length us, event | category | flops | bytes accessed | tf_op | source)
XLA Modules:
  0.0 172.1 jit_solution(17661177951421966962)
XLA Ops:
  0.0 0.0 copy-start.1
  0.0 0.0 copy-start.2
  0.0 0.0 copy-start.3
  0.0 1.0 constant_dynamic-update-slice_fusion.5
  1.0 0.0 copy-start.4
  1.0 0.0 copy-start.5
  1.0 0.0 copy-start.6
  1.0 0.9 constant_dynamic-update-slice_fusion.4
  2.0 1.0 constant_dynamic-update-slice_fusion.3
  3.0 1.0 constant_dynamic-update-slice_fusion.2
  3.9 0.0 copy-done.1
  4.0 0.0 copy-done.2
  4.0 0.0 copy-start
  4.0 0.0 copy-done.3
  4.1 0.8 pad.8.w_gates
  4.9 0.0 copy-done.4
  4.9 0.6 pad.9.decay
  5.5 0.0 copy-done.5
  5.5 0.0 copy-done.6
  5.5 0.1 bitcast_maximum_fusion
  5.6 0.7 copy.20.gate_bias
  6.2 0.0 copy-done
  6.2 164.0 %shard_map.145 = bf16[256,1024]{1,0:T(8,128)(2,1)} custom-call(bf16[256,4096]{1,0:T(8,128)(2,1)} %tokens.1, f32[1,4096]{1,0:T(1,128)} %bitcast.11, bf16[512,1280]{1,0:T(8,128)(2,1)} %copy-done, bf16[256,1024]{1,0:T(8,128)(2,1)} %wo_own.1, bf16[8,4096]{1,0:T(8,128)(2,1)} %pad.8.w_gates, f32[8,1]{1,0:T(8,128)} %copy.20.gate_bias, f32[8,256]{1,0:T(8,128)} %pad.9.decay, ...), custom_call_target="tpu_custom_call" | custom-call | tf_op jit(solution)/shard_map/pallas_call | solution.py:380
  170.3 1.9 %copy.30 = bf16[256,1024]{1,0:T(8,128)(2,1)} copy(bf16[256,1024]{1,0:T(8,128)(2,1)} %shard_map.145) | data formatting | bytes 1048576
  (6 shorter events, 0.1 us)
Async XLA Ops:
  0.0 3.9 %copy-start.1 = (bf16[512,256]{1,0:T(8,128)(2,1)S(1)}, bf16[512,256]{1,0:T(8,128)(2,1)}, u32[]{:S(2)}) copy-start(bf16[512,256]{1,0:T(8,128)(2,1)} %param.26) | copy-start | bytes 786436
  0.0 4.0 %copy-start.2 = (bf16[512,256]{1,0:T(8,128)(2,1)S(1)}, bf16[512,256]{1,0:T(8,128)(2,1)}, u32[]{:S(2)}) copy-start(bf16[512,256]{1,0:T(8,128)(2,1)} %param.27) | copy-start | bytes 786436
  0.0 4.0 %copy-start.3 = (bf16[4096,2,2,1]{0,2,3,1:T(2,128)(2,1)S(1)}, bf16[4096,2,2,1]{0,2,3,1:T(2,128)(2,1)}, u32[]{:S(2)}) copy-start(bf16[4096,2,2,1]{0,2,3,1:T(2,128)(2,1)} %param.20) | copy-start | bytes 98308
  1.0 3.9 %copy-start.4 = (f32[2,256,1]{1,2,0:T(1,128)S(1)}, f32[2,256,1]{1,2,0:T(1,128)}, u32[]{:S(2)}) copy-start(f32[2,256,1]{1,2,0:T(1,128)} %param.23) | copy-start | bytes 6148
  1.0 4.5 %copy-start.5 = (f32[2,1]{0,1:T(1,128)S(1)}, f32[2,1]{0,1:T(1,128)}, u32[]{:S(2)}) copy-start(f32[2,1]{0,1:T(1,128)} %param.22) | copy-start | bytes 28
  1.0 4.5 %copy-start.6 = (f32[2,1]{0,1:T(1,128)S(1)}, f32[2,1]{0,1:T(1,128)}, u32[]{:S(2)}) copy-start(f32[2,1]{0,1:T(1,128)} %param.21) | copy-start | bytes 28
  4.0 2.2 %copy-start = (bf16[512,1280]{1,0:T(8,128)(2,1)}, bf16[512,1280]{1,0:T(8,128)(2,1)S(1)}, u32[]{:S(2)}) copy-start(bf16[512,1280]{1,0:T(8,128)(2,1)S(1)} %constant_dynamic-update-slice_fusion.w_own) | copy-start | bytes 3932164

commit v3 on v2

--- a/solution.py
+++ b/solution.py
@@ -35,8 +35,8 @@
     return (1 - late) * (2 * place) + late * (2 * (n - 1 - place) + 1)
 
 
-def pieces(own):
-    return max(1, min(PIECES, own.shape[0] // 16))
+def pieces(depth):
+    return max(1, min(PIECES, depth // 16))
 
 
 def kernel(
@@ -46,11 +46,17 @@
     dv,
     tokens,
     norm_gain,
-    w_own,
-    wo_own,
+    w_query,
+    w_key,
+    w_value,
+    w_conv_b,
+    w_conv_c,
+    w_conv_in,
+    w_out,
     w_gates,
-    gate_bias,
-    decay,
+    input_bias,
+    forget_bias,
+    decay_shift,
     head_gain,
     taps,
     out,
@@ -75,6 +81,9 @@
     pk_rs,
     j_ss,
     j_rs,
+    own_sem,
+    gate_bias,
+    decay,
 ):
     me = lax.axis_index("sp")
     head = lax.axis_index("tp")
@@ -83,6 +92,20 @@
     left = ring_index(lax.rem(place + n - 1, n), n)
     rows = tokens.shape[0]
 
+    parts = (w_query, w_key, w_value, w_conv_b, w_conv_c, w_conv_in)
+    copies = []
+    offset = 0
+    for part in parts:
+        depth, cols = part.shape
+        spot = w_all.at[pl.ds(pl.multiple_of(me * depth, depth), depth), pl.ds(offset, cols)]
+        copies.append(pltpu.make_async_copy(part, spot, own_sem.at[len(copies)]))
+        offset += cols
+    depth_o = w_out.shape[0]
+    spot = wo_all.at[pl.ds(pl.multiple_of(me * depth_o, depth_o), depth_o), :]
+    copies.append(pltpu.make_async_copy(w_out, spot, own_sem.at[len(copies)]))
+    for copy in copies:
+        copy.start()
+
     barrier = pltpu.get_barrier_semaphore()
 
     def greet_sp(o, c):
@@ -97,15 +120,15 @@
     lax.fori_loop(1, t, greet_tp, 0)
     pl.semaphore_wait(barrier, n + t - 2)
 
-    def hop(own, whole, ss, rs, way, step, piece, first):
-        depth, width = own.shape
-        half, tall = width // 2, depth // pieces(own)
+    def hop(depth, whole, ss, rs, way, step, piece):
+        width = whole.shape[1]
+        half, tall = width // 2, depth // pieces(depth)
         holder = ring_index(lax.rem(place + (n + step if way else n - step), n), n)
         columns = pl.ds(way * half, half)
         there = whole.at[pl.ds(pl.multiple_of(holder * depth + piece * tall, tall), tall), columns]
-        turn = step * pieces(own) + piece
+        turn = step * pieces(depth) + piece
         return pltpu.make_async_remote_copy(
-            src_ref=own.at[pl.ds(piece * tall, tall), columns] if first else there,
+            src_ref=there,
             dst_ref=there,
             send_sem=ss.at[way, turn],
             recv_sem=rs.at[way, turn],
@@ -115,36 +138,39 @@
     def ring_start(*ring):
         for piece in range(pieces(ring[0])):
             for way in range(2):
-                hop(*ring, way, 0, piece, True).start()
+                hop(*ring, way, 0, piece).start()
 
     def ring_step(step, *ring):
         for piece in range(pieces(ring[0])):
             for way in range(2):
-                hop(*ring, way, step - 1, piece, False).wait_recv()
-                hop(*ring, way, step, piece, False).start()
+                hop(*ring, way, step - 1, piece).wait_recv()
+                hop(*ring, way, step, piece).start()
 
     def ring_last(*ring):
         for piece in range(pieces(ring[0])):
             for way in range(2):
-                hop(*ring, way, n - 2, piece, False).wait_recv()
+                hop(*ring, way, n - 2, piece).wait_recv()
 
     def ring_drain(*ring):
         def drain(step, c):
             for piece in range(pieces(ring[0])):
                 for way in range(2):
-                    hop(*ring, way, step, piece, False).wait_send()
+                    hop(*ring, way, step, piece).wait_send()
             return c
 
         lax.fori_loop(0, n - 1, drain, 0)
 
-    w_ring = (w_own, w_all, w_ss, w_rs)
-    wo_ring = (wo_own, wo_all, wo_ss, wo_rs)
+    w_ring = (w_query.shape[0], w_all, w_ss, w_rs)
+    wo_ring = (depth_o, wo_all, wo_ss, wo_rs)
+    for copy in copies:
+        copy.wait()
     ring_start(*w_ring)
 
-    depth = w_own.shape[0]
-    w_all[pl.ds(pl.multiple_of(me * depth, depth), depth), :] = w_own[...]
-    depth_o = wo_own.shape[0]
-    wo_all[pl.ds(pl.multiple_of(me * depth_o, depth_o), depth_o), :] = wo_own[...]
+    gate_bias[...] = jnp.zeros_like(gate_bias)
+    gate_bias[0:2, :] = input_bias[...]
+    gate_bias[2:4, :] = forget_bias[...]
+    decay[...] = jnp.zeros_like(decay)
+    decay[2:4, :] = decay_shift[...]
 
     chunk = 32
 
@@ -184,7 +210,7 @@
         proj[:, span] = dot(normed[...], w_all[:, span], NN).astype(BF16)
         return c
 
-    lax.fori_loop(0, w_own.shape[1] // width, project, 0)
+    lax.fori_loop(0, proj.shape[1] // width, project, 0)
 
     query = proj[:, :dk]
     keys = proj[:, dk : 2 * dk]
@@ -369,22 +395,21 @@
 ):
     rows, model = tokens.shape
     dk, dv = w_query.shape[1], w_value.shape[1]
-    w_own = jnp.concatenate([w_query, w_key, w_value, w_conv_b, w_conv_c, w_conv_in], axis=1)
     gates = jnp.transpose(w_gates[..., 0], (2, 1, 0)).reshape(4, model)
     gates = jnp.pad(gates, ((0, 4), (0, 0)))
-    bias = jnp.concatenate([input_bias, forget_bias, jnp.zeros((4, 1), F32)], axis=0)
-    decay = jnp.pad(decay_shift[..., 0], ((2, 4), (0, 0)))
-    wide, cols = w_own.shape[1], w_out.shape[1]
+    depth = w_query.shape[0]
+    wide, cols = 2 * dk + dv + 3 * w_conv_b.shape[1], w_out.shape[1]
+    hbm = pl.BlockSpec(memory_space=pl.ANY)
     vmem = pl.BlockSpec(memory_space=pltpu.VMEM)
     dma = pltpu.SemaphoreType.DMA
     return pl.pallas_call(
         functools.partial(kernel, n, t, dk, dv),
         out_shape=jax.ShapeDtypeStruct((rows, cols), BF16),
-        in_specs=[vmem] * 9,
+        in_specs=[vmem] * 2 + [hbm] * 7 + [vmem] * 6,
         out_specs=vmem,
         scratch_shapes=[
             pltpu.VMEM((rows, model), BF16),
-            pltpu.VMEM((n * w_own.shape[0], wide), BF16),
+            pltpu.VMEM((n * depth, wide), BF16),
             pltpu.VMEM((n * w_out.shape[0], cols), BF16),
             pltpu.VMEM((rows, wide), BF16),
             pltpu.VMEM((2, dk, dv), BF16),
@@ -394,16 +419,19 @@
             pltpu.VMEM((dk, dv), F32),
             pltpu.VMEM((1, dv), F32),
             pltpu.VMEM((t, rows, 2 * dv), BF16),
-            dma((2, (n - 1) * pieces(w_own))),
-            dma((2, (n - 1) * pieces(w_own))),
-            dma((2, (n - 1) * pieces(w_out))),
-            dma((2, (n - 1) * pieces(w_out))),
+            dma((2, (n - 1) * pieces(depth))),
+            dma((2, (n - 1) * pieces(depth))),
+            dma((2, (n - 1) * pieces(w_out.shape[0]))),
+            dma((2, (n - 1) * pieces(w_out.shape[0]))),
             dma((n,)),
             dma((n,)),
             dma((n,)),
             dma((n,)),
             dma((2, t)),
             dma((2, t)),
+            dma((7,)),
+            pltpu.VMEM((8, 1), F32),
+            pltpu.VMEM((8, rows), F32),
         ],
         compiler_params=pltpu.CompilerParams(
             collective_id=0, has_side_effects=True, vmem_limit_bytes=60 * 1024 * 1024
@@ -411,11 +439,17 @@
     )(
         tokens,
         norm_gain.reshape(1, model),
-        w_own,
+        w_query,
+        w_key,
+        w_value,
+        w_conv_b,
+        w_conv_c,
+        w_conv_in,
         w_out,
         gates,
-        bias,
-        decay,
+        input_bias,
+        forget_bias,
+        decay_shift[..., 0],
         head_gain.reshape(1, dv),
         conv_taps,
     )

time: 172 us -> 171 us (level)
    unnamed x21 -> x4, local copies, waits for them, and re-layouts: 5.8 us -> 5.73 us
where the time goes in v3:
time: 171 us
  Pallas kernels  164 us (96%)
  local copies, waits for them, and re-layouts  7.19 us (4%)
    pallas_call x1, Pallas kernels, body(): pl.pallas_call(functools.partial(kernel, n, t, dk, dv), out_shape=jax.Sha...  164 us
    unnamed x4, local copies, waits for them, and re-layouts  5.73 us

profile of v3, /device:TPU:0, one launch (start us, length us, event | category | flops | bytes accessed | tf_op | source)
XLA Modules:
  0.0 170.8 jit_solution(8219512467109546086)
XLA Ops:
  0.0 1.3 copy.17.input_bias
  1.3 1.3 copy.18.forget_bias
  2.6 1.3 copy.21
  3.9 0.8 copy.16
  4.7 0.6 pad.4.w_gates
  5.3 163.6 %shard_map.145 = bf16[256,1024]{1,0:T(8,128)(2,1)} custom-call(bf16[256,4096]{1,0:T(8,128)(2,1)} %tokens.1, f32[1,4096]{1,0:T(1,128)} %bitcast.9, bf16[512,128]{1,0:T(8,128)(2,1)} %w_query.1, bf16[512,128]{1,0:T(8,128)(2,1)} %w_key.1, bf16[512,256]{1,0:T(8,128)(2,1)} %w_value.1, bf16[512,256]{1,0:T(8,128)(2,1)} %w_conv_b.1, bf16[512,256]{1,0:T(8,128)(2,1)} %w_conv_c.1, ...), custom_call_target="tpu_custom_call" | custom-call | tf_op jit(solution)/shard_map/pallas_call | solution.py:405
  168.9 1.9 %copy.23 = bf16[256,1024]{1,0:T(8,128)(2,1)} copy(bf16[256,1024]{1,0:T(8,128)(2,1)} %shard_map.145) | data formatting | bytes 1048576
  (1 shorter events, 0.0 us)

commit v4 on v3

--- a/solution.py
+++ b/solution.py
@@ -10,7 +10,7 @@
 EPS = 1e-06
 HIGH = lax.Precision.HIGHEST
 LOWEST = -1e30
-PIECES = 4
+PIECES = 8
 F32 = jnp.float32
 BF16 = jnp.bfloat16
 

time: 171 us -> 172 us (level)
  no operation moved by 1% of the time
where the time goes in v4:
time: 172 us
  Pallas kernels  165 us (96%)
  local copies, waits for them, and re-layouts  7.19 us (4%)
    pallas_call x1, Pallas kernels, body(): pl.pallas_call(functools.partial(kernel, n, t, dk, dv), out_shape=jax.Sha...  165 us
    unnamed x4, local copies, waits for them, and re-layouts  5.73 us

profile of v4, /device:TPU:0, one launch (start us, length us, event | category | flops | bytes accessed | tf_op | source)
XLA Modules:
  0.0 171.9 jit_solution(15645480221620683010)
XLA Ops:
  0.0 1.3 copy.17.input_bias
  1.3 1.3 copy.18.forget_bias
  2.6 1.3 copy.21
  3.9 0.8 copy.16
  4.7 0.6 pad.4.w_gates
  5.3 164.7 %shard_map.145 = bf16[256,1024]{1,0:T(8,128)(2,1)} custom-call(bf16[256,4096]{1,0:T(8,128)(2,1)} %tokens.1, f32[1,4096]{1,0:T(1,128)} %bitcast.9, bf16[512,128]{1,0:T(8,128)(2,1)} %w_query.1, bf16[512,128]{1,0:T(8,128)(2,1)} %w_key.1, bf16[512,256]{1,0:T(8,128)(2,1)} %w_value.1, bf16[512,256]{1,0:T(8,128)(2,1)} %w_conv_b.1, bf16[512,256]{1,0:T(8,128)(2,1)} %w_conv_c.1, ...), custom_call_target="tpu_custom_call" | custom-call | tf_op jit(solution)/shard_map/pallas_call | solution.py:405
  170.0 1.9 %copy.23 = bf16[256,1024]{1,0:T(8,128)(2,1)} copy(bf16[256,1024]{1,0:T(8,128)(2,1)} %shard_map.145) | data formatting | bytes 1048576
  (1 shorter events, 0.0 us)
